TPU v7x, 32 devices: a whole 2x2x4 slice. The times are simulated.
32 devices in a mesh: sp: 16 (over z, y, x), tp: 2 (over core).
Axes of the slice: x: 2, y: 2, z: 4, core: 2. Of those that a mesh axis runs over, the one named last changes fastest.
Arguments:
- queries: bfloat16 [6144, 2048], P('sp', 'tp'), may hold values from -6 to 6
- key_heads: bfloat16 [6144, 1024], P('sp', 'tp'), may hold values from -6 to 6
- value_heads: bfloat16 [6144, 1024], P('sp', 'tp'), may hold values from -6 to 6
- sink_logit: float32 [16], P('tp'), may hold values from 3 to 7
- doc_ids: int32 [6144], replicated, may hold values from 0 to 3, never falling along the last dimension, each value on 1 to 3072 neighbouring positions
- residual: bfloat16 [6144, 2048], P('sp'), may hold values from -6 to 6
- out_proj: bfloat16 [2048, 2048], P('tp'), may hold values from -0.125 to 0.125
- gain_mix: float32 [2048], replicated, may hold values from 0.1 to 1.9
- up_proj: bfloat16 [2048, 8192], P('sp', 'tp'), may hold values from -0.125 to 0.125
- down_proj: bfloat16 [8192, 2048], P('tp', 'sp'), may hold values from -0.0625 to 0.0625
- gain_ffn_in: float32 [2048], replicated, may hold values from 0.1 to 1.9
- gain_ffn_out: float32 [2048], replicated, may hold values from 0.1 to 1.9
Outputs:
- layer_out: bfloat16 [6144, 2048], P(('sp', 'tp'))
All inputs are finite; a program needn't handle non-finite values.
Results may differ from a plain program's by a relative error of at most 0.019.
Values may be sent and summed in bfloat16 or wider, within the bound.
A program may use at most 128 MiB of HBM per device.

v0:
```python
import jax
import jax.numpy as jnp
from jax import lax
from jax.sharding import PartitionSpec as P

HD = 128
WINDOW = 128


def padded(shard, sides, width):
    for axis, dim in sides:
        devices, length = (lax.axis_size(axis), shard.shape[dim])
        up = [(i, (i + 1) % devices) for i in range(devices - 1)]
        down = [(j, i) for i, j in up]
        last = lax.slice_in_dim(shard, length - width, length, axis=dim)
        first = lax.slice_in_dim(shard, 0, width, axis=dim)
        before = lax.ppermute(last, axis, up)
        after = lax.ppermute(first, axis, down)
        shard = jnp.concatenate([before, shard, after], axis=dim)
    return shard


def rotate(field, places):
    half_dim = HD // 2
    inv_freq = 10000.0 ** (-jnp.arange(0, HD, 2, dtype=jnp.float32) / HD)
    angles = places[:, None, None] * inv_freq[None, None, :]
    cosine = jnp.cos(angles)
    sine = jnp.sin(angles)
    lower = field[..., :half_dim].astype(jnp.float32)
    upper = field[..., half_dim:].astype(jnp.float32)
    return jnp.concatenate(
        [lower * cosine - upper * sine, upper * cosine + lower * sine], axis=-1
    ).astype(jnp.bfloat16)


def banded(field, blocks):
    framed = field.reshape((blocks + 2, WINDOW) + field.shape[1:])
    return jnp.concatenate([framed[:-2], framed[1:-1], framed[2:]], axis=1)


def rms_scale(field, gain_vec):
    return field * lax.rsqrt(jnp.mean(field * field, axis=-1, keepdims=True) + 1e-06) * gain_vec


def body(
    queries,
    key_heads,
    value_heads,
    sink_logit,
    doc_ids,
    residual,
    out_proj,
    gain_mix,
    up_proj,
    down_proj,
    gain_ffn_in,
    gain_ffn_out,
):
    tok_count = queries.shape[0]
    blocks = tok_count // WINDOW
    share_rows = tok_count // lax.axis_size("tp")
    q_local = queries.shape[1] // HD
    kv_local = key_heads.shape[1] // HD
    group_size = q_local // kv_local
    offset = lax.axis_index("sp") * tok_count
    places = (offset + jnp.arange(tok_count)).astype(jnp.float32)
    rotated_q = rotate(queries.reshape(tok_count, q_local, HD), places).reshape(
        blocks, WINDOW, kv_local, group_size, HD
    )
    rotated_k = rotate(key_heads.reshape(tok_count, kv_local, HD), places).reshape(
        tok_count, kv_local * HD
    )
    rimmed = padded(jnp.stack([rotated_k, value_heads]), (("sp", 1),), WINDOW)
    key_win = banded(rimmed[0].reshape(-1, kv_local, HD), blocks)
    val_win = banded(rimmed[1].reshape(-1, kv_local, HD), blocks)
    padded_docs = jnp.pad(doc_ids, (WINDOW, WINDOW), constant_values=-1)
    key_docs = banded(lax.dynamic_slice_in_dim(padded_docs, offset, tok_count + 2 * WINDOW), blocks)
    query_docs = lax.dynamic_slice_in_dim(doc_ids, offset, tok_count).reshape(blocks, WINDOW)
    q_index = jnp.arange(WINDOW)[:, None]
    k_index = jnp.arange(3 * WINDOW)[None, :]
    in_window = jnp.abs(k_index - WINDOW - q_index) <= WINDOW
    allowed = (in_window[None] & (query_docs[:, :, None] == key_docs[:, None, :]))[:, None, None]
    scores = jnp.einsum(
        "nqkgd,nskd->nkgqs", rotated_q, key_win, preferred_element_type=jnp.float32
    ) * HD ** (-0.5)
    masked = jnp.where(allowed, scores, -1e30)
    sink_col = sink_logit.reshape(kv_local, group_size)[None, :, :, None]
    top_score = jnp.maximum(jnp.max(masked, axis=-1), sink_col)
    exp_scores = jnp.where(allowed, jnp.exp(masked - top_score[..., None]), 0.0)
    denom_sum = jnp.sum(exp_scores, axis=-1) + jnp.exp(sink_col - top_score)
    probs = (exp_scores / denom_sum[..., None]).astype(jnp.bfloat16)
    attn = (
        jnp.einsum("nkgqs,nskd->nqkgd", probs, val_win, preferred_element_type=jnp.float32)
        .astype(jnp.bfloat16)
        .reshape(tok_count, q_local * HD)
    )
    mixed = lax.psum(
        jnp.dot(attn, out_proj, preferred_element_type=jnp.float32).astype(jnp.bfloat16), "tp"
    ).astype(jnp.float32)
    after_all = (residual.astype(jnp.float32) + rms_scale(mixed, gain_mix)).astype(jnp.bfloat16)
    normed = rms_scale(after_all.astype(jnp.float32), gain_ffn_in).astype(jnp.bfloat16)
    after_mix = lax.dynamic_slice_in_dim(
        after_all, lax.axis_index("tp") * share_rows, share_rows, 0
    )
    up_acts = jnp.dot(
        normed,
        lax.all_gather(up_proj, "sp", axis=0, tiled=True),
        preferred_element_type=jnp.float32,
    )
    hidden = jnp.square(jax.nn.relu(up_acts)).astype(jnp.bfloat16)
    partial_value = jnp.dot(
        hidden,
        lax.all_gather(down_proj, "sp", axis=1, tiled=True),
        preferred_element_type=jnp.float32,
    )
    ffn_out = lax.psum_scatter(
        partial_value.astype(jnp.bfloat16), "tp", scatter_dimension=0, tiled=True
    ).astype(jnp.float32)
    return (after_mix.astype(jnp.float32) + rms_scale(ffn_out, gain_ffn_out)).astype(jnp.bfloat16)


def solution(mesh):
    return jax.shard_map(
        body,
        mesh=mesh,
        in_specs=(
            P("sp", "tp"),
            P("sp", "tp"),
            P("sp", "tp"),
            P("tp"),
            P(),
            P("sp", None),
            P("tp", None),
            P(),
            P("sp", "tp"),
            P("tp", "sp"),
            P(),
            P(),
        ),
        out_specs=P(("sp", "tp"), None),
        check_vma=False,
    )
```

profile of v0, /device:TPU:0, one launch (start us, length us, event | category | flops | bytes accessed | tf_op | source)
XLA Modules:
  0.0 535.9 jit_solution(408335233760002139)
XLA Ops:
  7.4 1.3 copy.28
  8.7 1.2 copy.29
  11.3 5.6 %collective-permute-start = (bf16[2,128,512]{1,2,0:T(8,128)(2,1)}, bf16[2,128,512]{1,2,0:T(8,128)(2,1)}, u32[]{:S(2)}, u32[]{:S(2)}) collective-permute-start(bf16[2,128,512]{1,2,0:T(8,128)(2,1)} %get-tuple-element.15), channel_id=1, source_target_pairs={{0,2},{2,4},{4,6},{6,8},{8,10},{10,12},{12,14},{14,16},{16,18},{18... | collective-permute-start | bytes 786440 | tf_op jit(solution)/shard_map/ppermute | solution.py:17
  16.9 1.3 collective-permute-start.1
  20.3 1.2 copy.43
  21.6 1.2 copy.44
  23.6 1.0 copy.33
  24.8 2.9 collective-permute-done
  27.7 1.9 collective-permute-done.1
  29.6 1.3 pad_maximum_fusion.5
  31.8 2.4 fusion.1
  34.3 2.0 copy-done
  36.4 1.2 fusion.2
  38.1 4.0 fusion.24
  43.2 5.1 convolution_convert_fusion
  49.8 19.4 %all-reduce.3.cloned.1.call-done = bf16[384,2048]{1,0:T(8,128)(2,1)} async-done(((bf16[384,2048]{1,0:T(8,128)(2,1)}), bf16[384,2048]{1,0:T(8,128)(2,1)}) %all-reduce.3.cloned.1.call-update) | async-done | bytes 1572880 | tf_op jit(solution)/shard_map/psum | solution.py:97
  69.2 1.8 fusion.3
  71.0 2.3 fusion.7
  73.3 169.4 %all-gather.3.cloned.1.call-done = bf16[2048,4096]{1,0:T(8,128)(2,1)} async-done(((bf16[128,4096]{1,0:T(8,128)(2,1)}), bf16[2048,4096]{1,0:T(8,128)(2,1)}) %all-gather.3.cloned.1.call-update) | async-done | bytes 16777232 | tf_op jit(solution)/shard_map/all_gather | solution.py:107
  242.7 249.7 %all-gather.5.cloned.1.call-done = bf16[4096,2048]{1,0:T(8,128)(2,1)} async-done(((bf16[4096,128]{1,0:T(8,128)(2,1)}), bf16[4096,2048]{1,0:T(8,128)(2,1)}) %all-gather.5.cloned.1.call-update) | async-done | bytes 16777232 | tf_op jit(solution)/shard_map/all_gather | solution.py:113
  492.4 24.9 %fusion.11 = bf16[384,2048]{1,0:T(8,128)(2,1)} fusion(bf16[4096,2048]{1,0:T(8,128)(2,1)} %all-gather.5.cloned.1.call-done, bf16[2048,4096]{1,0:T(8,128)(2,1)} %all-gather.3.cloned.1.call-done, bf16[384,2048]{1,0:T(8,128)(2,1)S(1)} %get-tuple-element.6, f32[2048]{0:T(1024)S(1)} %copy-done.11, f32[384]{0:T(512)S(1)} %add_rsqrt_fusion), kind=kOutput, calls=%fused_computation.19 | convolution fusion | flops 12893552640 | bytes 36709888 | tf_op jit(solution)/shard_map/dot_general | solution.py:111
  517.4 7.4 %reduce-scatter.2.cloned.1.call-done = bf16[192,2048]{1,0:T(8,128)(2,1)} async-done(((bf16[384,2048]{1,0:T(8,128)(2,1)}), bf16[192,2048]{1,0:T(8,128)(2,1)}) %reduce-scatter.2.cloned.1.call-update) | async-done | bytes 786448 | tf_op jit(solution)/shard_map/reduce_scatter | solution.py:116
  524.7 1.4 fusion.13
  526.1 2.4 fusion.16
  (66 shorter events, 8.5 us)
Async XLA Ops:
  7.4 10.8 %copy-start.6 = (s32[6144]{0:T(1024)S(1)}, s32[6144]{0:T(1024)}, u32[]{:S(2)}) copy-start(s32[6144]{0:T(1024)} %param.16) | copy-start | bytes 73732
  7.4 11.0 %copy-start.3 = (bf16[384,1024]{1,0:T(8,128)(2,1)S(1)}, bf16[384,1024]{1,0:T(8,128)(2,1)}, u32[]{:S(2)}) copy-start(bf16[384,1024]{1,0:T(8,128)(2,1)} %param.12) | copy-start | bytes 2359300
  7.4 61.8 %all-reduce.3.cloned.1.call-start = ((), (), s32[]{:S(2)}) async-start(), calls=%async_computation.1 | async-start | bytes 3145728 | tf_op jit(solution)/shard_map/psum | solution.py:97
  10.5 9.6 %copy-start.1 = (bf16[384,512]{1,0:T(8,128)(2,1)S(1)}, bf16[384,512]{1,0:T(8,128)(2,1)}, u32[]{:S(2)}) copy-start(bf16[384,512]{1,0:T(8,128)(2,1)} %param.14) | copy-start | bytes 1179652
  11.3 16.3 %collective-permute-start = (bf16[2,128,512]{1,2,0:T(8,128)(2,1)}, bf16[2,128,512]{1,2,0:T(8,128)(2,1)}, u32[]{:S(2)}, u32[]{:S(2)}) collective-permute-start(bf16[2,128,512]{1,2,0:T(8,128)(2,1)} %get-tuple-element.15), channel_id=1, source_target_pairs={{0,2},{2,4},{4,6},{6,8},{8,10},{10,12},{12,14},{14,16},{16,18},{18... | collective-permute-start | bytes 786440 | tf_op jit(solution)/shard_map/ppermute | solution.py:17
  16.9 12.7 %collective-permute-start.1 = (bf16[2,128,512]{1,2,0:T(8,128)(2,1)S(1)}, bf16[2,128,512]{1,2,0:T(8,128)(2,1)}, u32[]{:S(2)}, u32[]{:S(2)}) collective-permute-start(bf16[2,128,512]{1,2,0:T(8,128)(2,1)S(1)} %get-tuple-element.16), channel_id=1, source_target_pairs={{2,0},{4,2},{6,4},{8,6},{10,8},{12,10},{14,12},{16,14},{18,16},{20... | collective-permute-start | bytes 786440 | tf_op jit(solution)/shard_map/ppermute | solution.py:18
  19.0 3.8 copy-start.10
  24.7 7.0 %copy-start.4 = (bf16[3,128,4,2,64]{4,1,3,2,0:T(8,128)(2,1)S(1)}, bf16[3,128,4,2,64]{4,1,3,2,0:T(8,128)(2,1)}, u32[]{:S(2)}) copy-start(bf16[3,128,4,2,64]{4,1,3,2,0:T(8,128)(2,1)} %copy.43) | copy-start | bytes 1179652
  31.8 2.5 copy-start.7
  34.2 2.1 copy-start
  36.4 1.7 copy-start.5
  48.4 22.6 %copy-start.2 = (bf16[384,2048]{1,0:T(8,128)(2,1)S(1)}, bf16[384,2048]{1,0:T(8,128)(2,1)}, u32[]{:S(2)}) copy-start(bf16[384,2048]{1,0:T(8,128)(2,1)} %param.17) | copy-start | bytes 4718596
  48.4 22.6 %copy-start.8 = (f32[2048]{0:T(1024)S(1)}, f32[2048]{0:T(1024)}, u32[]{:S(2)}) copy-start(f32[2048]{0:T(1024)} %param.19) | copy-start | bytes 24580
  48.4 194.3 %all-gather.3.cloned.1.call-start = ((), (), s32[]{:S(2)}) async-start(), calls=%async_computation.2 | async-start | bytes 17825792 | tf_op jit(solution)/shard_map/all_gather | solution.py:107
  49.0 443.5 %all-gather.5.cloned.1.call-start = ((), (), s32[]{:S(2)}) async-start(), calls=%async_computation.3 | async-start | bytes 17825792 | tf_op jit(solution)/shard_map/all_gather | solution.py:113
  49.5 442.9 %copy-start.11 = (f32[2048]{0:T(1024)S(1)}, f32[2048]{0:T(1024)}, u32[]{:S(2)}) copy-start(f32[2048]{0:T(1024)} %param.22) | copy-start | bytes 24580
  49.6 475.2 %reduce-scatter.2.cloned.1.call-start = ((), (), s32[]{:S(2)}) async-start(), calls=%async_computation.4 | async-start | bytes 2359296 | tf_op jit(solution)/shard_map/reduce_scatter | solution.py:116
  492.4 33.7 %copy-start.9 = (f32[2048]{0:T(1024)S(1)}, f32[2048]{0:T(1024)}, u32[]{:S(2)}) copy-start(f32[2048]{0:T(1024)} %param.23) | copy-start | bytes 24580
Sparse Core Ops, SparseCore 0:
  48.5 20.6 all-reduce.2
  517.5 7.2 reduce-scatter.1
Sparse Core Ops, SparseCore 1:
  51.6 191.0 all-gather.2
  245.3 247.1 all-gather.4
where the time goes:
time: 536 us
  waiting for transfers between devices  452 us (84%)
  matrix products  36.4 us (7%)
  between operations  15.2 us (3%)
  local copies, waits for them, and re-layouts  12.9 us (2%)
  other arithmetic  12.5 us (2%)
  starting transfers between devices  7.15 us (1%)
    all_gather x1, waiting for transfers between devices, body(): lax.all_gather(down_proj, 'sp', axis=1, tiled=True)  250 us
    all_gather x1, waiting for transfers between devices, body(): lax.all_gather(up_proj, 'sp', axis=0, tiled=True)  169 us
    dot_general x1, matrix products, body(): jnp.dot(hidden, lax.all_gather(down_proj, 'sp', axis=1, tiled=True), pref...  24.9 us
    psum x1, waiting for transfers between devices, body(): lax.psum(jnp.dot(attn, out_proj, preferred_element_type=jnp.float32).asty...  19.4 us
  transfers between devices with their start and end apart: 6, of which 6 were waited for; matrix products, arithmetic and copies ran while one was open for 2% of the time, Pallas kernels for 0%

commit v1 on v0

--- a/solution.py
+++ b/solution.py
@@ -110,7 +110,7 @@
     hidden = jnp.square(jax.nn.relu(up_acts)).astype(jnp.bfloat16)
     partial_value = jnp.dot(
         hidden,
-        lax.all_gather(down_proj, "sp", axis=1, tiled=True),
+        jnp.concatenate(lax.all_gather(down_proj, "sp"), axis=1),
         preferred_element_type=jnp.float32,
     )
     ffn_out = lax.psum_scatter(

time: 536 us -> 473 us (0.88)
  waiting for transfers between devices: 452 us -> 372 us
  local copies, waits for them, and re-layouts: 12.9 us -> 34.3 us
  matrix products: 36.4 us -> 30.3 us
    all_gather x1, waiting for transfers between devices: 250 us -> 169 us  [body(): lax.all_gather(down_proj, 'sp')]
    reshape x0 -> x1, local copies, waits for them, and re-layouts: none -> 21.4 us  [body(): jnp.concatenate(lax.all_gather(down_proj, 'sp'), axis=1)]
    dot_general x1, matrix products: 24.9 us -> 18.8 us  [body(): jnp.dot(hidden, jnp.concatenate(lax.all_gather(down_proj, 'sp'), axis=1),...]
  transfers between devices with their start and end apart: 6 -> 6, of which waited for: 6 -> 6; matrix products, arithmetic and copies ran while one was open for 2% -> 7% of each run, Pallas kernels for 0% -> 0%
where the time goes in v1:
time: 473 us; the launch traced here: 472 us
  waiting for transfers between devices  372 us (79%)
  local copies, waits for them, and re-layouts  34.3 us (7%)
  matrix products  30.3 us (6%)
  between operations  15.2 us (3%)
  other arithmetic  13.1 us (3%)
  starting transfers between devices  7.15 us (2%)
    all_gather x1, waiting for transfers between devices, body(): lax.all_gather(up_proj, 'sp', axis=0, tiled=True)  170 us
    all_gather x1, waiting for transfers between devices, body(): lax.all_gather(down_proj, 'sp')  169 us
    reshape x1, local copies, waits for them, and re-layouts, body(): jnp.concatenate(lax.all_gather(down_proj, 'sp'), axis=1)  21.4 us
    psum x1, waiting for transfers between devices, body(): lax.psum(jnp.dot(attn, out_proj, preferred_element_type=jnp.float32).asty...  19.4 us
    dot_general x1, matrix products, body(): jnp.dot(hidden, jnp.concatenate(lax.all_gather(down_proj, 'sp'), axis=1),...  18.8 us
  transfers between devices with their start and end apart: 6, of which 6 were waited for; matrix products, arithmetic and copies ran while one was open for 7% of the time, Pallas kernels for 0%

profile of v1, /device:TPU:0, one launch (start us, length us, event | category | flops | bytes accessed | tf_op | source)
XLA Modules:
  0.0 471.7 jit_solution(55040648973050308)
XLA Ops:
  7.4 1.3 copy.28
  8.7 1.2 copy.29
  11.3 5.6 %collective-permute-start = (bf16[2,128,512]{1,2,0:T(8,128)(2,1)}, bf16[2,128,512]{1,2,0:T(8,128)(2,1)}, u32[]{:S(2)}, u32[]{:S(2)}) collective-permute-start(bf16[2,128,512]{1,2,0:T(8,128)(2,1)} %get-tuple-element.15), channel_id=1, source_target_pairs={{0,2},{2,4},{4,6},{6,8},{8,10},{10,12},{12,14},{14,16},{16,18},{18... | collective-permute-start | bytes 786440 | tf_op jit(solution)/shard_map/ppermute | solution.py:17
  16.9 1.3 collective-permute-start.1
  20.9 1.3 copy.43
  22.3 1.2 copy.44
  25.4 2.3 collective-permute-done
  27.7 1.9 collective-permute-done.1
  29.6 1.3 pad_maximum_fusion.5
  31.8 2.4 fusion
  34.3 2.0 copy-done
  36.4 1.2 fusion.1
  38.1 4.0 fusion.23
  43.2 5.1 %convolution_convert_fusion = bf16[384,2048]{1,0:T(8,128)(2,1)} fusion(bf16[384,1024]{1,0:T(8,128)(2,1)S(1)} %reshape.209, bf16[1024,2048]{1,0:T(8,128)(2,1)} %param.18), kind=kOutput, calls=%fused_computation.19 | convolution fusion | flops 1611399168 | bytes 6553600 | tf_op jit(solution)/shard_map/dot_general | solution.py:98
  49.8 19.4 %all-reduce.3.cloned.1.call-done = bf16[384,2048]{1,0:T(8,128)(2,1)} async-done(((bf16[384,2048]{1,0:T(8,128)(2,1)}), bf16[384,2048]{1,0:T(8,128)(2,1)}) %all-reduce.3.cloned.1.call-update) | async-done | bytes 1572880 | tf_op jit(solution)/shard_map/psum | solution.py:97
  69.2 1.8 fusion.2
  71.0 2.3 fusion.6
  73.3 169.4 %all-gather.6.cloned.1.call-done = bf16[65536,128]{1,0:T(8,128)(2,1)} async-done(((bf16[4096,128]{1,0:T(8,128)(2,1)}), bf16[65536,128]{1,0:T(8,128)(2,1)}) %all-gather.6.cloned.1.call-update) | async-done | bytes 16777232 | tf_op jit(solution)/shard_map/all_gather | solution.py:113
  242.7 21.4 %copy.47 = bf16[4096,16,128]{0,2,1:T(8,128)(2,1)} copy(bf16[4096,16,128]{2,0,1:T(8,128)(2,1)} %bitcast.62) | data formatting | bytes 33554432 | tf_op jit(solution)/shard_map/reshape | solution.py:113
  264.1 170.2 %all-gather.4.cloned.1.call-done = bf16[2048,4096]{1,0:T(8,128)(2,1)} async-done(((bf16[128,4096]{1,0:T(8,128)(2,1)}), bf16[2048,4096]{1,0:T(8,128)(2,1)}) %all-gather.4.cloned.1.call-update) | async-done | bytes 16777232 | tf_op jit(solution)/shard_map/all_gather | solution.py:107
  434.3 18.8 %fusion.10 = bf16[384,2048]{1,0:T(8,128)(2,1)} fusion(bf16[4096,2048]{0,1:T(8,128)(2,1)} %bitcast.63, bf16[2048,4096]{1,0:T(8,128)(2,1)} %all-gather.4.cloned.1.call-done, bf16[384,2048]{1,0:T(8,128)(2,1)S(1)} %get-tuple-element.6, f32[2048]{0:T(1024)S(1)} %copy-done.12, f32[384]{0:T(512)S(1)} %add_rsqrt_fusion), kind=kOutput, calls=%fused_computation.18 | convolution fusion | flops 12893552640 | bytes 36709888 | tf_op jit(solution)/shard_map/dot_general | solution.py:111
  453.1 7.4 %reduce-scatter.2.cloned.1.call-done = bf16[192,2048]{1,0:T(8,128)(2,1)} async-done(((bf16[384,2048]{1,0:T(8,128)(2,1)}), bf16[192,2048]{1,0:T(8,128)(2,1)}) %reduce-scatter.2.cloned.1.call-update) | async-done | bytes 786448 | tf_op jit(solution)/shard_map/reduce_scatter | solution.py:116
  460.5 1.4 fusion.12
  461.9 2.4 fusion.15
  (69 shorter events, 10.1 us)
Async XLA Ops:
  7.4 10.8 %copy-start.7 = (s32[6144]{0:T(1024)S(1)}, s32[6144]{0:T(1024)}, u32[]{:S(2)}) copy-start(s32[6144]{0:T(1024)} %param.16) | copy-start | bytes 73732
  7.4 11.6 %copy-start.3 = (bf16[384,1024]{1,0:T(8,128)(2,1)S(1)}, bf16[384,1024]{1,0:T(8,128)(2,1)}, u32[]{:S(2)}) copy-start(bf16[384,1024]{1,0:T(8,128)(2,1)} %param.12) | copy-start | bytes 2359300
  7.4 61.8 %all-reduce.3.cloned.1.call-start = ((), (), s32[]{:S(2)}) async-start(), calls=%async_computation.1 | async-start | bytes 3145728 | tf_op jit(solution)/shard_map/psum | solution.py:97
  10.5 10.2 %copy-start.1 = (bf16[384,512]{1,0:T(8,128)(2,1)S(1)}, bf16[384,512]{1,0:T(8,128)(2,1)}, u32[]{:S(2)}) copy-start(bf16[384,512]{1,0:T(8,128)(2,1)} %param.14) | copy-start | bytes 1179652
  11.3 16.3 %collective-permute-start = (bf16[2,128,512]{1,2,0:T(8,128)(2,1)}, bf16[2,128,512]{1,2,0:T(8,128)(2,1)}, u32[]{:S(2)}, u32[]{:S(2)}) collective-permute-start(bf16[2,128,512]{1,2,0:T(8,128)(2,1)} %get-tuple-element.15), channel_id=1, source_target_pairs={{0,2},{2,4},{4,6},{6,8},{8,10},{10,12},{12,14},{14,16},{16,18},{18... | collective-permute-start | bytes 786440 | tf_op jit(solution)/shard_map/ppermute | solution.py:17
  16.9 12.7 %collective-permute-start.1 = (bf16[2,128,512]{1,2,0:T(8,128)(2,1)S(1)}, bf16[2,128,512]{1,2,0:T(8,128)(2,1)}, u32[]{:S(2)}, u32[]{:S(2)}) collective-permute-start(bf16[2,128,512]{1,2,0:T(8,128)(2,1)S(1)} %get-tuple-element.16), channel_id=1, source_target_pairs={{2,0},{4,2},{6,4},{8,6},{10,8},{12,10},{14,12},{16,14},{18,16},{20... | collective-permute-start | bytes 786440 | tf_op jit(solution)/shard_map/ppermute | solution.py:18
  19.6 3.9 copy-start.11
  20.7 4.5 copy-start.6
  25.4 6.4 %copy-start.4 = (bf16[3,128,4,2,64]{4,1,3,2,0:T(8,128)(2,1)S(1)}, bf16[3,128,4,2,64]{4,1,3,2,0:T(8,128)(2,1)}, u32[]{:S(2)}) copy-start(bf16[3,128,4,2,64]{4,1,3,2,0:T(8,128)(2,1)} %copy.43) | copy-start | bytes 1179652
  31.8 2.5 copy-start.8
  34.2 2.1 copy-start
  36.4 1.7 copy-start.5
  48.4 22.6 %copy-start.2 = (bf16[384,2048]{1,0:T(8,128)(2,1)S(1)}, bf16[384,2048]{1,0:T(8,128)(2,1)}, u32[]{:S(2)}) copy-start(bf16[384,2048]{1,0:T(8,128)(2,1)} %param.17) | copy-start | bytes 4718596
  48.4 22.6 %copy-start.9 = (f32[2048]{0:T(1024)S(1)}, f32[2048]{0:T(1024)}, u32[]{:S(2)}) copy-start(f32[2048]{0:T(1024)} %param.19) | copy-start | bytes 24580
  48.4 194.3 %all-gather.6.cloned.1.call-start = ((), (), s32[]{:S(2)}) async-start(), calls=%async_computation.4 | async-start | bytes 17825792 | tf_op jit(solution)/shard_map/all_gather | solution.py:113
  49.0 385.3 %all-gather.4.cloned.1.call-start = ((), (), s32[]{:S(2)}) async-start(), calls=%async_computation.2 | async-start | bytes 17825792 | tf_op jit(solution)/shard_map/all_gather | solution.py:107
  49.6 410.9 %reduce-scatter.2.cloned.1.call-start = ((), (), s32[]{:S(2)}) async-start(), calls=%async_computation.3 | async-start | bytes 2359296 | tf_op jit(solution)/shard_map/reduce_scatter | solution.py:116
  242.7 191.6 %copy-start.12 = (f32[2048]{0:T(1024)S(1)}, f32[2048]{0:T(1024)}, u32[]{:S(2)}) copy-start(f32[2048]{0:T(1024)} %param.22) | copy-start | bytes 24580
  434.3 27.6 %copy-start.10 = (f32[2048]{0:T(1024)S(1)}, f32[2048]{0:T(1024)}, u32[]{:S(2)}) copy-start(f32[2048]{0:T(1024)} %param.23) | copy-start | bytes 24580
Sparse Core Ops, SparseCore 0:
  48.5 20.6 all-reduce.2
  453.2 7.2 reduce-scatter.1
Sparse Core Ops, SparseCore 1:
  51.6 191.0 all-gather.5
  245.3 188.9 all-gather.3
